TPU v7x, 256 devices: a whole 4x4x8 slice. The times are simulated.
256 devices in a mesh: rep: 2 (over z_hi), fs: 16 (over z_lo, y), tp: 8 (over x, core).
Axes of the slice: x: 4, y: 4, z: 8 (z_hi: 2, z_lo: 4; z = z_hi * 4 + z_lo), core: 2. Of those that a mesh axis runs over, the one named last changes fastest.
Arguments:
- stream: bfloat16 [32768, 2048], P(('rep', 'fs', 'tp')), may hold values from -6 to 6
- gain_before: float32 [2048], replicated, may hold values from 0.1 to 1.9
- gain_after: float32 [2048], replicated, may hold values from 0.1 to 1.9
- proj_gate: bfloat16 [2048, 3584], P('fs', 'tp'), may hold values from -0.125 to 0.125
- proj_lift: bfloat16 [2048, 3584], P('fs', 'tp'), may hold values from -0.125 to 0.125
- proj_down: bfloat16 [3584, 2048], P('tp', 'fs'), may hold values from -0.09375 to 0.09375
- mixer_gain: float32 [2048], replicated, may hold values from 0.1 to 1.9
- mixer_u: bfloat16 [2048, 2048], P('fs', 'tp'), may hold values from -0.125 to 0.125
- mixer_v: bfloat16 [2048, 2048], P('fs', 'tp'), may hold values from -1 to 1
- layer_gain: float32 [2048], P('tp'), may hold values from 0.1 to 1.9
- layer_shift: float32 [2048], P('tp'), may hold values from -3 to 3
- spatial: bfloat16 [16, 128, 128], P('tp'), may hold values from -0.5 to 0.5
- spatial_shift: float32 [16, 128], P('tp'), may hold values from 0.2 to 2
- mixer_down: bfloat16 [2048, 2048], P('tp', 'fs'), may hold values from -0.125 to 0.125
Outputs:
- result: bfloat16 [32768, 2048], P(('rep', 'fs', 'tp'))
All inputs are finite; a program needn't handle non-finite values.
Results may differ from a plain program's by a relative error of at most 0.017.
Values may be sent and summed in bfloat16 or wider, within the bound.
A program may use at most 128 MiB of HBM per device.

v0:
```python
import jax
import jax.numpy as jnp
from jax import lax
from jax.sharding import PartitionSpec as P

GROUP_DIM = 128
SPAN = 128
A = 2048
norm_epsilon = 1e-06
layer_epsilon = 1e-05


def sent_to_all(value, axis):
    copies = jnp.broadcast_to(value, (lax.axis_size(axis), *value.shape))
    return lax.all_to_all(copies, axis, split_axis=0, concat_axis=0, tiled=True)


def laid_out(tiles, dim):
    lengths = list(tiles.shape[1:])
    lengths[dim] *= tiles.shape[0]
    return jnp.moveaxis(tiles, 0, dim).reshape(lengths)


def gathered_copies(value, axis, dim):
    tiles = sent_to_all(value, axis)
    return laid_out(tiles, dim)


def side_by_side(arrays, axis, dim, along):
    ends, at = ([], 0)
    for a in arrays[:-1]:
        at += a.shape[along]
        ends.append(at)
    both = jnp.concatenate(arrays, axis=along)
    return tuple(jnp.split(lax.all_gather(both, axis, axis=dim, tiled=True), ends, axis=along))


def norm_rows(row_block, scale_gain):
    widened = row_block.astype(jnp.float32)
    factor = lax.rsqrt(jnp.mean(widened * widened, axis=1, keepdims=True) + norm_epsilon)
    return (widened * factor * scale_gain).astype(jnp.bfloat16)


def gathered_norm(stream_rows, scale_gain):
    gathered = lax.all_gather(stream_rows, "tp", axis=0, tiled=True)
    return norm_rows(gathered, scale_gain)


def pair_adder(normed, pieces):
    return (
        jnp.dot(normed, pieces[0], preferred_element_type=jnp.float32),
        jnp.dot(normed, pieces[1], preferred_element_type=jnp.float32),
    )


def activate(gate_vals, lift_vals):
    return (jax.nn.silu(gate_vals) * lift_vals).astype(jnp.bfloat16)


def rows_project(columns_here, weight_shard):
    weight_cols = gathered_copies(weight_shard, "fs", 1)
    weight_whole = lax.all_gather(weight_cols, "tp", axis=0, tiled=True)
    own_tokens = lax.all_to_all(columns_here, "tp", split_axis=0, concat_axis=1, tiled=True)
    width = columns_here.shape[1]
    running = jnp.zeros((own_tokens.shape[0], weight_whole.shape[1]), jnp.float32)
    for member in range(lax.axis_size("tp")):
        partial_value = jnp.dot(
            own_tokens[:, member * width : (member + 1) * width],
            weight_whole[member * width : (member + 1) * width],
            preferred_element_type=jnp.float32,
        )
        running = running + partial_value.astype(jnp.bfloat16).astype(jnp.float32)
    return running


def half_kept(stream_rows, scale_gain, gate_whole, lift_whole, proj_down):
    normed = gathered_norm(stream_rows, scale_gain)
    gate_vals = jnp.dot(normed, gate_whole, preferred_element_type=jnp.float32)
    lift_vals = jnp.dot(normed, lift_whole, preferred_element_type=jnp.float32)
    hidden = activate(gate_vals, lift_vals)
    summed = rows_project(hidden, proj_down)
    return (stream_rows.astype(jnp.float32) + 0.5 * summed).astype(jnp.bfloat16)


def token_mixer(
    stream_rows,
    mixer_gain,
    mixer_u,
    mixer_v,
    layer_gain,
    layer_shift,
    spatial,
    spatial_shift,
    mixer_down,
):
    gathered = lax.all_gather(stream_rows, "tp", axis=0, tiled=True)
    normed = norm_rows(gathered, mixer_gain)
    seq_tokens = normed.shape[0]
    u_vals, v_vals = pair_adder(normed, side_by_side((mixer_u, mixer_v), "fs", 0, 1))
    lifted = jax.nn.gelu(v_vals)
    moments = lax.psum((jnp.sum(lifted, axis=1), jnp.sum(lifted * lifted, axis=1)), "tp")
    centre = moments[0] / A
    spread = moments[1] / A - centre * centre
    normed_v = (
        (lifted - centre[:, None]) * lax.rsqrt(spread[:, None] + layer_epsilon) * layer_gain
        + layer_shift
    ).astype(jnp.bfloat16)
    groups_here = spatial.shape[0]
    blocked = normed_v.reshape(seq_tokens // SPAN, SPAN, groups_here, GROUP_DIM)
    causal = jnp.tril(jnp.ones((SPAN, SPAN), dtype=bool))
    masked = jnp.where(causal[None], spatial, jnp.zeros((), jnp.bfloat16))
    mixed_v = jnp.einsum("gts,bsgd->btgd", masked, blocked, preferred_element_type=jnp.float32)
    mixed_v = mixed_v + spatial_shift.T[None, :, :, None]
    gated = (jax.nn.gelu(u_vals) * mixed_v.reshape(seq_tokens, groups_here * GROUP_DIM)).astype(
        jnp.bfloat16
    )
    summed = rows_project(gated, mixer_down)
    return (stream_rows.astype(jnp.float32) + summed).astype(jnp.bfloat16)


def body(
    stream,
    gain_before,
    gain_after,
    proj_gate,
    proj_lift,
    proj_down,
    mixer_gain,
    mixer_u,
    mixer_v,
    layer_gain,
    layer_shift,
    spatial,
    spatial_shift,
    mixer_down,
):
    gate_whole, lift_whole = side_by_side((proj_gate, proj_lift), "fs", 0, 1)
    first = half_kept(stream, gain_before, gate_whole, lift_whole, proj_down)
    second = token_mixer(
        first,
        mixer_gain,
        mixer_u,
        mixer_v,
        layer_gain,
        layer_shift,
        spatial,
        spatial_shift,
        mixer_down,
    )
    result = half_kept(second, gain_after, gate_whole, lift_whole, proj_down)
    return result


def solution(mesh):
    placed = (
        P(("rep", "fs", "tp"), None),
        P(),
        P(),
        P("fs", "tp"),
        P("fs", "tp"),
        P("tp", "fs"),
        P(),
        P("fs", "tp"),
        P("fs", "tp"),
        P("tp"),
        P("tp"),
        P("tp", None, None),
        P("tp", None),
        P("tp", "fs"),
    )
    return jax.shard_map(
        body, mesh=mesh, in_specs=placed, out_specs=P(("rep", "fs", "tp"), None), check_vma=False
    )
```

profile of v0, /device:TPU:1, one launch (start us, length us, event | category | flops | bytes accessed | tf_op | source)
XLA Modules:
  0.0 495.1 jit_solution(2137628182025998506)
XLA Ops:
  10.3 51.8 %all_to_all.68 = bf16[16,448,128]{2,1,0:T(8,128)(2,1)S(1)} all-to-all(bf16[16,448,128]{2,1,0:T(8,128)(2,1)S(1)} %broadcast_in_dim.14), channel_id=1, replica_groups=mesh['rep'=2,'fs'=16,'tp'=8] {'fs'}, dimensions={0} | all-to-all | bytes 3670016 | tf_op jit(solution)/shard_map/all_to_all | solution.py:15
  63.7 3.1 fusion
  66.8 58.1 %all-gather.10.cloned.1.call-done = bf16[2048,896]{0,1:T(8,128)(2,1)} async-done(((bf16[128,896]{0,1:T(8,128)(2,1)}), bf16[2048,896]{0,1:T(8,128)(2,1)}) %all-gather.10.cloned.1.call-update) | async-done | bytes 3670032 | tf_op jit(solution)/shard_map/all_gather | solution.py:35
  124.9 5.1 %fusion.80 = f32[1024,448]{0,1:T(8,128)S(1)} fusion(bf16[2048,896]{0,1:T(8,128)(2,1)} %all-gather.10.cloned.1.call-done, bf16[1024,2048]{1,0:T(8,128)(2,1)} %all-gather.8.cloned.1.call-done, f32[2048]{0:T(1024)S(1)} %copy-done.16, f32[1024]{0:T(1024)S(1)} %add_rsqrt_fusion.3), kind=kOutput, calls=%fused_computation.113 | convolution fusion | flops 1887436800 | bytes 7876608 | tf_op jit(solution)/shard_map/dot_general | solution.py:79
  130.0 2.5 fusion.91
  132.7 34.0 %all_to_all.69 = bf16[8,128,448]{1,2,0:T(8,128)(2,1)S(1)} all-to-all(bf16[8,128,448]{1,2,0:T(8,128)(2,1)S(1)} %bitcast.46), channel_id=1, replica_groups=mesh['rep'=2,'fs'=16,'tp'=8] {'tp'}, dimensions={0} | all-to-all | bytes 1835008 | tf_op jit(solution)/shard_map/all_to_all | solution.py:63
  166.8 54.7 %all-gather.12.cloned.1.call-done = bf16[3584,2048]{1,0:T(8,128)(2,1)} async-done(((bf16[448,2048]{1,0:T(8,128)(2,1)}), bf16[3584,2048]{1,0:T(8,128)(2,1)}) %all-gather.12.cloned.1.call-update) | async-done | bytes 14680080 | tf_op jit(solution)/shard_map/all_gather | solution.py:62
  221.4 2.1 fusion.61
  223.5 2.4 fusion.60
  225.9 2.6 fusion.58
  234.4 32.1 %all_to_all.70 = bf16[16,256,128]{1,2,0:T(8,128)(2,1)} all-to-all(bf16[16,256,128]{1,2,0:T(8,128)(2,1)S(1)} %broadcast_in_dim.21), channel_id=1, replica_groups=mesh['rep'=2,'fs'=16,'tp'=8] {'fs'}, dimensions={0} | all-to-all | bytes 2097152 | tf_op jit(solution)/shard_map/all_to_all | solution.py:15
  266.6 3.1 fusion.3
  269.7 70.9 %all-gather.16.cloned.1.call-done = bf16[2048,512]{1,0:T(8,128)(2,1)} async-done(((bf16[128,512]{1,0:T(8,128)(2,1)}), bf16[2048,512]{1,0:T(8,128)(2,1)}) %all-gather.16.cloned.1.call-update) | async-done | bytes 2097168 | tf_op jit(solution)/shard_map/all_gather | solution.py:35
  340.6 4.1 fusion.169
  344.7 22.8 %all-reduce = (f32[1024]{0:T(1024)S(1)}, f32[1024]{0:T(1024)S(1)}) all-reduce(f32[1024]{0:T(1024)S(1)} %get-tuple-element.6, f32[1024]{0:T(1024)S(1)} %get-tuple-element.5), channel_id=1, replica_groups=mesh['rep'=2,'fs'=16,'tp'=8] {'tp'}, use_global_device_ids=true, to_apply=%region_5.6 | all-reduce | flops 2048 | bytes 16384 | tf_op jit(solution)/shard_map/psum | solution.py:101
  369.0 4.0 fusion.117
  374.1 4.1 all-to-all-start.2
  378.2 34.6 %all-gather.18.cloned.1.call-done = bf16[2048,2048]{0,1:T(8,128)(2,1)} async-done(((bf16[256,2048]{0,1:T(8,128)(2,1)}), bf16[2048,2048]{0,1:T(8,128)(2,1)}) %all-gather.18.cloned.1.call-update) | async-done | bytes 8388624 | tf_op jit(solution)/shard_map/all_gather | solution.py:62
  414.7 2.1 fusion.42
  421.9 34.6 %all-gather.20.cloned.1.call-done = bf16[1024,2048]{1,0:T(8,128)(2,1)} async-done(((bf16[128,2048]{1,0:T(8,128)(2,1)}), bf16[1024,2048]{1,0:T(8,128)(2,1)}) %all-gather.20.cloned.1.call-update) | async-done | bytes 4194320 | tf_op jit(solution)/shard_map/all_gather | solution.py:45
  456.5 3.2 fusion.6
  459.9 4.0 fusion.78
  464.0 2.6 fusion.94
  466.8 16.7 %all_to_all.71 = bf16[8,128,448]{1,2,0:T(8,128)(2,1)S(1)} all-to-all(bf16[8,128,448]{1,2,0:T(8,128)(2,1)S(1)} %bitcast.47), channel_id=1, replica_groups=mesh['rep'=2,'fs'=16,'tp'=8] {'tp'}, dimensions={0} | all-to-all | bytes 1835008 | tf_op jit(solution)/shard_map/all_to_all | solution.py:63
  (102 shorter events, 25.7 us)
Async XLA Ops:
  6.5 57.1 %all-gather.8.cloned.1.call-start = ((), (), s32[]{:S(2)}) async-start(), calls=%async_computation.5 | async-start | bytes 4718592 | tf_op jit(solution)/shard_map/all_gather | solution.py:45
  7.3 117.6 %all-gather.10.cloned.1.call-start = ((), (), s32[]{:S(2)}) async-start(), calls=%async_computation.6 | async-start | bytes 3899392 | tf_op jit(solution)/shard_map/all_gather | solution.py:35
  9.0 212.4 %all-gather.12.cloned.1.call-start = ((), (), s32[]{:S(2)}) async-start(), calls=%async_computation.7 | async-start | bytes 16515072 | tf_op jit(solution)/shard_map/all_gather | solution.py:62
  62.1 62.8 %copy-start.16 = (f32[2048]{0:T(1024)S(1)}, f32[2048]{0:T(1024)}, u32[]{:S(2)}) copy-start(f32[2048]{0:T(1024)} %param.15) | copy-start | bytes 24580
  63.6 203.0 %all-gather.14.cloned.1.call-start = ((), (), s32[]{:S(2)}) async-start(), calls=%async_computation.8 | async-start | bytes 4718592 | tf_op jit(solution)/shard_map/all_gather | solution.py:96
  124.9 5.1 %copy-start.4 = (bf16[1024,2048]{1,0:T(8,128)(2,1)S(1)}, bf16[1024,2048]{1,0:T(8,128)(2,1)}, u32[]{:S(2)}) copy-start(bf16[1024,2048]{1,0:T(8,128)(2,1)} %all-gather.8.cloned.1.call-done) | copy-start | bytes 12582916
  124.9 5.1 %copy-start.14 = (bf16[2048,896]{0,1:T(8,128)(2,1)S(1)}, bf16[2048,896]{0,1:T(8,128)(2,1)}, u32[]{:S(2)}) copy-start(bf16[2048,896]{0,1:T(8,128)(2,1)} %all-gather.10.cloned.1.call-done) | copy-start | bytes 11010052
  221.4 9.1 %copy-start = (bf16[3584,2048]{1,0:T(8,128)(2,1)S(1)}, bf16[3584,2048]{1,0:T(8,128)(2,1)}, u32[]{:S(2)}) copy-start(bf16[3584,2048]{1,0:T(8,128)(2,1)} %all-gather.12.cloned.1.call-done) | copy-start | bytes 44040196
  233.4 107.2 %all-gather.16.cloned.1.call-start = ((), (), s32[]{:S(2)}) async-start(), calls=%async_computation.9 | async-start | bytes 2228224 | tf_op jit(solution)/shard_map/all_gather | solution.py:35
  234.1 178.7 %all-gather.18.cloned.1.call-start = ((), (), s32[]{:S(2)}) async-start(), calls=%async_computation.10 | async-start | bytes 9437184 | tf_op jit(solution)/shard_map/all_gather | solution.py:62
  234.3 106.3 %copy-start.17 = (f32[2048]{0:T(1024)S(1)}, f32[2048]{0:T(1024)}, u32[]{:S(2)}) copy-start(f32[2048]{0:T(1024)} %param.20) | copy-start | bytes 24580
  269.6 97.9 %copy-start.11 = (f32[256]{0:T(256)S(1)}, f32[256]{0:T(256)}, u32[]{:S(2)}) copy-start(f32[256]{0:T(256)} %param.24) | copy-start | bytes 3076
  269.7 97.9 %copy-start.12 = (f32[256]{0:T(256)S(1)}, f32[256]{0:T(256)}, u32[]{:S(2)}) copy-start(f32[256]{0:T(256)} %param.23) | copy-start | bytes 3076
  269.7 98.4 %copy-start.7 = (bf16[2,128,128]{2,1,0:T(8,128)(2,1)S(1)}, bf16[2,128,128]{2,1,0:T(8,128)(2,1)}, u32[]{:S(2)}) copy-start(bf16[2,128,128]{2,1,0:T(8,128)(2,1)} %param.25) | copy-start | bytes 196612
  269.7 98.3 %copy-start.13 = (f32[2,128]{1,0:T(2,128)S(1)}, f32[2,128]{1,0:T(2,128)}, u32[]{:S(2)}) copy-start(f32[2,128]{1,0:T(2,128)} %param.26) | copy-start | bytes 3076
  374.1 38.7 %all-to-all-start.2 = ((bf16[8,128,256]{1,2,0:T(8,128)(2,1)}), bf16[8,128,256]{1,2,0:T(8,128)(2,1)S(1)}, u32[]{:S(2)}, u32[]{:S(2)}) async-start(bf16[8,128,256]{1,2,0:T(8,128)(2,1)} %copy.42), calls=%async_computation.2 | async-start | bytes 1048576 | tf_op jit(solution)/shard_map/all_to_all | solution.py:63
  378.2 78.3 %all-gather.20.cloned.1.call-start = ((), (), s32[]{:S(2)}) async-start(), calls=%async_computation.11 | async-start | bytes 4718592 | tf_op jit(solution)/shard_map/all_gather | solution.py:45
  412.8 5.7 %copy-start.1 = (bf16[2048,2048]{0,1:T(8,128)(2,1)S(1)}, bf16[2048,2048]{0,1:T(8,128)(2,1)}, u32[]{:S(2)}) copy-start(bf16[2048,2048]{0,1:T(8,128)(2,1)} %all-gather.18.cloned.1.call-done) | copy-start | bytes 25165828
  420.5 39.2 %copy-start.18 = (f32[2048]{0:T(1024)S(1)}, f32[2048]{0:T(1024)}, u32[]{:S(2)}) copy-start(f32[2048]{0:T(1024)} %param.16) | copy-start | bytes 24580
  459.9 4.0 copy-start.15
  459.9 23.5 %slice-start = ((s8[14680064]{0:T(1024)(128)(4,1)}), s8[4194304]{0:T(1024)(128)(4,1)S(1)}, s32[]{:S(2)}) async-start(s8[14680064]{0:T(1024)(128)(4,1)} %bitcast.43), calls=%async_computation.12 | async-start | bytes 8388608
  459.9 23.5 %slice-start.1 = ((s8[14680064]{0:T(1024)(128)(4,1)}), s8[4194304]{0:T(1024)(128)(4,1)S(1)}, s32[]{:S(2)}) async-start(s8[14680064]{0:T(1024)(128)(4,1)} %bitcast.43), calls=%async_computation.13 | async-start | bytes 8388608
  463.9 19.5 %slice-start.2 = ((s8[14680064]{0:T(1024)(128)(4,1)}), s8[4194304]{0:T(1024)(128)(4,1)S(1)}, s32[]{:S(2)}) async-start(s8[14680064]{0:T(1024)(128)(4,1)} %bitcast.43), calls=%async_computation.14 | async-start | bytes 8388608
  464.0 19.5 %slice-start.3 = ((s8[14680064]{0:T(1024)(128)(4,1)}), s8[2097152]{0:T(1024)(128)(4,1)S(1)}, s32[]{:S(2)}) async-start(s8[14680064]{0:T(1024)(128)(4,1)} %bitcast.43), calls=%async_computation.15 | async-start | bytes 4194304
  (7 other events, 13.5 us)
Sparse Core Ops, SparseCore 0:
  9.2 38.7 all-gather.7
  49.7 75.1 all-gather.9
  126.7 94.6 all-gather.11
  233.5 33.0 all-gather.13
  268.2 72.3 all-gather.15
  342.2 70.5 all-gather.17
  422.0 34.4 all-gather.19
where the time goes:
time: 496 us; the launch traced here: 495 us
  waiting for transfers between devices  254 us (51%)
  blocking collectives  157 us (32%)
  matrix products  48 us (10%)
  between operations  14 us (3%)
  other arithmetic  12.1 us (2%)
  local copies, waits for them, and re-layouts  5.48 us (1%)
    all_gather x2, waiting for transfers between devices, side_by_side(): lax.all_gather(both, axis, axis=dim, tiled=True)  129 us
    all_gather x2, waiting for transfers between devices, rows_project(): weight_whole = lax.all_gather(weight_cols, 'tp', axis=0, tiled=True)  89.3 us
    all_to_all x2, blocking collectives, sent_to_all(): return lax.all_to_all(copies, axis, split_axis=0, concat_axis=0, tiled=True)  83.9 us
    all_to_all x2, blocking collectives, rows_project(): lax.all_to_all(columns_here, 'tp', split_axis=0, concat_axis=1, tiled=True)  50.8 us
    all_gather x2, waiting for transfers between devices, gathered_norm(): gathered = lax.all_gather(stream_rows, 'tp', axis=0, tiled=True)  34.6 us
    dot_general x24, matrix products, rows_project(): jnp.dot(own_tokens[:, member * width:(member + 1) * width], weight_whole[...  25.3 us
    psum x1, blocking collectives, token_mixer(): lax.psum((jnp.sum(lifted, axis=1), jnp.sum(lifted * lifted, axis=1)), 'tp')  22.8 us
  transfers between devices with their start and end apart: 8, of which 5 were waited for; matrix products, arithmetic and copies ran while one was open for 6% of the time, Pallas kernels for 0%

commit v1 on v0

--- a/solution.py
+++ b/solution.py
@@ -8,6 +8,12 @@
 A = 2048
 norm_epsilon = 1e-06
 layer_epsilon = 1e-05
+
+
+def tiled_gather(x, axis, dim):
+    length = lax.axis_size(axis)
+    repeats = [length if d == dim else 1 for d in range(x.ndim)]
+    return lax.all_to_all(jnp.tile(x, repeats), axis, split_axis=dim, concat_axis=dim, tiled=True)
 
 
 def sent_to_all(value, axis):
@@ -59,7 +65,7 @@
 
 def rows_project(columns_here, weight_shard):
     weight_cols = gathered_copies(weight_shard, "fs", 1)
-    weight_whole = lax.all_gather(weight_cols, "tp", axis=0, tiled=True)
+    weight_whole = tiled_gather(weight_cols, "tp", 0)
     own_tokens = lax.all_to_all(columns_here, "tp", split_axis=0, concat_axis=1, tiled=True)
     width = columns_here.shape[1]
     running = jnp.zeros((own_tokens.shape[0], weight_whole.shape[1]), jnp.float32)

time: 496 us -> 585 us (1.18)
  blocking collectives: 157 us -> 249 us
  waiting for transfers between devices: 254 us -> 215 us
  starting transfers between devices: 4.31 us -> 32.2 us
  local copies, waits for them, and re-layouts: 5.48 us -> 17.4 us
    all_to_all x0 -> x1, blocking collectives: none -> 165 us  [tiled_gather(): lax.all_to_all(jnp.tile(x, repeats), axis, split_axis=dim, concat_axis=di...]
    all_gather x2 -> x0, waiting for transfers between devices: 89.3 us -> none  [rows_project(): weight_whole = lax.all_gather(weight_cols, 'tp', axis=0, tiled=True)]
    all_to_all x2 -> x1, blocking collectives: 83.9 us -> 31.1 us  [sent_to_all(): return lax.all_to_all(copies, axis, split_axis=0, concat_axis=0, tiled=True)]
    all_gather x2, waiting for transfers between devices: 34.6 us -> 58.6 us  [gathered_norm(): gathered = lax.all_gather(stream_rows, 'tp', axis=0, tiled=True)]
    all_to_all x2, blocking collectives: 50.8 us -> 29.5 us  [rows_project(): lax.all_to_all(columns_here, 'tp', split_axis=0, concat_axis=1, tiled=True)]
    all_to_all x0 -> x2, starting transfers between devices: none -> 17 us  [the longest x1 9.31 us: sent_to_all(): return lax.all_to_all(copies, axis, split_axis=0, concat_axis=0, tiled=True)]
    all_gather x2, waiting for transfers between devices: 129 us -> 144 us  [side_by_side(): lax.all_gather(both, axis, axis=dim, tiled=True)]
    all_to_all x1, waiting for transfers between devices: 0.01 us -> 12 us  [rows_project(): lax.all_to_all(columns_here, 'tp', split_axis=0, concat_axis=1, tiled=True)]
where the time goes in v1:
time: 585 us; the launch traced here: 584 us
  blocking collectives  249 us (43%)
  waiting for transfers between devices  215 us (37%)
  matrix products  45.3 us (8%)
  starting transfers between devices  32.2 us (6%)
  local copies, waits for them, and re-layouts  17.4 us (3%)
  between operations  13.6 us (2%)
  other arithmetic  12.1 us (2%)
    all_to_all x1, blocking collectives, tiled_gather(): lax.all_to_all(jnp.tile(x, repeats), axis, split_axis=dim, concat_axis=di...  165 us
    all_gather x2, waiting for transfers between devices, side_by_side(): lax.all_gather(both, axis, axis=dim, tiled=True)  144 us
    all_gather x2, waiting for transfers between devices, gathered_norm(): gathered = lax.all_gather(stream_rows, 'tp', axis=0, tiled=True)  58.6 us
    all_to_all x1, blocking collectives, sent_to_all(): return lax.all_to_all(copies, axis, split_axis=0, concat_axis=0, tiled=True)  31.1 us
    all_to_all x2, blocking collectives, rows_project(): lax.all_to_all(columns_here, 'tp', split_axis=0, concat_axis=1, tiled=True)  29.5 us
    psum x1, blocking collectives, token_mixer(): lax.psum((jnp.sum(lifted, axis=1), jnp.sum(lifted * lifted, axis=1)), 'tp')  23.6 us
    dot_general x24, matrix products, rows_project(): jnp.dot(own_tokens[:, member * width:(member + 1) * width], weight_whole[...  22.6 us
    all_to_all x1, starting transfers between devices, rows_project(): lax.all_to_all(columns_here, 'tp', split_axis=0, concat_axis=1, tiled=True)  14.9 us
  transfers between devices with their start and end apart: 8, of which 5 were waited for; matrix products, arithmetic and copies ran while one was open for 6% of the time, Pallas kernels for 0%

profile of v1, /device:TPU:1, one launch (start us, length us, event | category | flops | bytes accessed | tf_op | source)
XLA Modules:
  0.0 584.4 jit_solution(6432731403862925931)
XLA Ops:
  11.5 9.3 %all-to-all-start.1 = ((bf16[16,448,128]{2,1,0:T(8,128)(2,1)}), bf16[16,448,128]{2,1,0:T(8,128)(2,1)S(1)}, u32[]{:S(2)}, u32[]{:S(2)}) async-start(bf16[16,448,128]{2,1,0:T(8,128)(2,1)} %broadcast_in_dim.14), calls=%async_computation.1 | async-start | bytes 3670016 | tf_op jit(solution)/shard_map/all_to_all | solution.py:21
  20.8 27.2 %all-gather.6.cloned.1.call-done = bf16[1024,2048]{1,0:T(8,128)(2,1)} async-done(((bf16[128,2048]{1,0:T(8,128)(2,1)}), bf16[1024,2048]{1,0:T(8,128)(2,1)}) %all-gather.6.cloned.1.call-update) | async-done | bytes 4194320 | tf_op jit(solution)/shard_map/all_gather | solution.py:51
  48.0 3.1 fusion
  51.1 74.4 %all-gather.8.cloned.1.call-done = bf16[2048,896]{0,1:T(8,128)(2,1)} async-done(((bf16[128,896]{0,1:T(8,128)(2,1)}), bf16[2048,896]{0,1:T(8,128)(2,1)}) %all-gather.8.cloned.1.call-update) | async-done | bytes 3670032 | tf_op jit(solution)/shard_map/all_gather | solution.py:41
  125.5 5.1 fusion.64
  130.6 2.5 fusion.75
  134.2 14.9 %all-to-all-start = ((bf16[8,128,448]{1,2,0:T(8,128)(2,1)}), bf16[8,128,448]{1,2,0:T(8,128)(2,1)S(1)}, u32[]{:S(2)}, u32[]{:S(2)}) async-start(bf16[8,128,448]{1,2,0:T(8,128)(2,1)} %bitcast.98), calls=%async_computation | async-start | bytes 1835008 | tf_op jit(solution)/shard_map/all_to_all | solution.py:69
  150.7 12.0 %all-to-all-done = bf16[8,128,448]{1,2,0:T(8,128)(2,1)S(1)} async-done(((bf16[8,128,448]{1,2,0:T(8,128)(2,1)}), bf16[8,128,448]{1,2,0:T(8,128)(2,1)S(1)}, u32[]{:S(2)}, u32[]{:S(2)}) %all-to-all-start) | async-done | bytes 917536 | tf_op jit(solution)/shard_map/all_to_all | solution.py:69
  162.7 3.7 tile.9
  166.4 164.7 %all_to_all.81 = bf16[8,448,2048]{2,1,0:T(8,128)(2,1)S(1)} all-to-all(bf16[8,448,2048]{2,1,0:T(8,128)(2,1)S(1)} %tile.9), channel_id=1, replica_groups=mesh['rep'=2,'fs'=16,'tp'=8] {'tp'}, dimensions={0} | all-to-all | bytes 29360128 | tf_op jit(solution)/shard_map/all_to_all | solution.py:16
  337.8 31.1 %all_to_all.82 = bf16[16,256,128]{1,2,0:T(8,128)(2,1)S(1)} all-to-all(bf16[16,256,128]{1,2,0:T(8,128)(2,1)S(1)} %broadcast_in_dim.21), channel_id=1, replica_groups=mesh['rep'=2,'fs'=16,'tp'=8] {'fs'}, dimensions={0} | all-to-all | bytes 2097152 | tf_op jit(solution)/shard_map/all_to_all | solution.py:21
  369.6 4.4 tile.11
  373.9 7.7 %all-to-all-start.5 = ((bf16[8,256,2048]{2,1,0:T(8,128)(2,1)}), bf16[8,256,2048]{2,1,0:T(8,128)(2,1)}, u32[]{:S(2)}, u32[]{:S(2)}) async-start(bf16[8,256,2048]{2,1,0:T(8,128)(2,1)} %tile.11), calls=%async_computation.5 | async-start | bytes 16777216 | tf_op jit(solution)/shard_map/all_to_all | solution.py:16
  382.6 3.1 fusion.3
  385.8 69.1 %all-gather.12.cloned.1.call-done = bf16[2048,512]{1,0:T(8,128)(2,1)} async-done(((bf16[128,512]{1,0:T(8,128)(2,1)}), bf16[2048,512]{1,0:T(8,128)(2,1)}) %all-gather.12.cloned.1.call-update) | async-done | bytes 2097168 | tf_op jit(solution)/shard_map/all_gather | solution.py:41
  454.9 4.1 fusion.145
  459.0 23.6 %all-reduce = (f32[1024]{0:T(1024)S(1)}, f32[1024]{0:T(1024)S(1)}) all-reduce(f32[1024]{0:T(1024)S(1)} %get-tuple-element.6, f32[1024]{0:T(1024)S(1)} %get-tuple-element.5), channel_id=1, replica_groups=mesh['rep'=2,'fs'=16,'tp'=8] {'tp'}, use_global_device_ids=true, to_apply=%region_5.6 | all-reduce | flops 2048 | bytes 16384 | tf_op jit(solution)/shard_map/psum | solution.py:107
  484.1 4.0 fusion.101
  488.4 12.8 %all_to_all.83 = bf16[8,128,256]{1,2,0:T(8,128)(2,1)S(1)} all-to-all(bf16[8,128,256]{1,2,0:T(8,128)(2,1)S(1)} %copy.43), channel_id=1, replica_groups=mesh['rep'=2,'fs'=16,'tp'=8] {'tp'}, dimensions={0} | all-to-all | bytes 1048576 | tf_op jit(solution)/shard_map/all_to_all | solution.py:69
  514.7 31.4 %all-gather.14.cloned.1.call-done = bf16[1024,2048]{1,0:T(8,128)(2,1)} async-done(((bf16[128,2048]{1,0:T(8,128)(2,1)}), bf16[1024,2048]{1,0:T(8,128)(2,1)}) %all-gather.14.cloned.1.call-update) | async-done | bytes 4194320 | tf_op jit(solution)/shard_map/all_gather | solution.py:51
  546.1 3.2 fusion.6
  549.5 4.0 fusion.62
  553.6 2.6 fusion.78
  556.4 16.7 %all_to_all.84 = bf16[8,128,448]{1,2,0:T(8,128)(2,1)S(1)} all-to-all(bf16[8,128,448]{1,2,0:T(8,128)(2,1)S(1)} %bitcast.102), channel_id=1, replica_groups=mesh['rep'=2,'fs'=16,'tp'=8] {'tp'}, dimensions={0} | all-to-all | bytes 1835008 | tf_op jit(solution)/shard_map/all_to_all | solution.py:69
  (101 shorter events, 36.0 us)
Async XLA Ops:
  6.5 41.5 %all-gather.6.cloned.1.call-start = ((), (), s32[]{:S(2)}) async-start(), calls=%async_computation.7 | async-start | bytes 4718592 | tf_op jit(solution)/shard_map/all_gather | solution.py:51
  7.3 118.2 %all-gather.8.cloned.1.call-start = ((), (), s32[]{:S(2)}) async-start(), calls=%async_computation.8 | async-start | bytes 3899392 | tf_op jit(solution)/shard_map/all_gather | solution.py:41
  11.5 113.9 %copy-start.15 = (f32[2048]{0:T(1024)S(1)}, f32[2048]{0:T(1024)}, u32[]{:S(2)}) copy-start(f32[2048]{0:T(1024)} %param.15) | copy-start | bytes 24580
  11.5 122.7 %all-to-all-start.1 = ((bf16[16,448,128]{2,1,0:T(8,128)(2,1)}), bf16[16,448,128]{2,1,0:T(8,128)(2,1)S(1)}, u32[]{:S(2)}, u32[]{:S(2)}) async-start(bf16[16,448,128]{2,1,0:T(8,128)(2,1)} %broadcast_in_dim.14), calls=%async_computation.1 | async-start | bytes 3670016 | tf_op jit(solution)/shard_map/all_to_all | solution.py:21
  125.5 5.1 copy-start.3
  125.5 5.1 copy-start.13
  134.2 28.5 %all-to-all-start = ((bf16[8,128,448]{1,2,0:T(8,128)(2,1)}), bf16[8,128,448]{1,2,0:T(8,128)(2,1)S(1)}, u32[]{:S(2)}, u32[]{:S(2)}) async-start(bf16[8,128,448]{1,2,0:T(8,128)(2,1)} %bitcast.98), calls=%async_computation | async-start | bytes 1835008 | tf_op jit(solution)/shard_map/all_to_all | solution.py:69
  149.1 233.5 %all-gather.10.cloned.1.call-start = ((), (), s32[]{:S(2)}) async-start(), calls=%async_computation.9 | async-start | bytes 4718592 | tf_op jit(solution)/shard_map/all_gather | solution.py:102
  331.1 5.2 copy-start
  373.9 7.7 %copy-start.8 = (bf16[128,256]{1,0:T(8,128)(2,1)S(1)}, bf16[128,256]{1,0:T(8,128)(2,1)}, u32[]{:S(2)}) copy-start(bf16[128,256]{1,0:T(8,128)(2,1)} %param.22) | copy-start | bytes 196612
  373.9 7.7 %copy-start.9 = (bf16[128,256]{1,0:T(8,128)(2,1)S(1)}, bf16[128,256]{1,0:T(8,128)(2,1)}, u32[]{:S(2)}) copy-start(bf16[128,256]{1,0:T(8,128)(2,1)} %param.21) | copy-start | bytes 196612
  373.9 114.5 %all-to-all-start.5 = ((bf16[8,256,2048]{2,1,0:T(8,128)(2,1)}), bf16[8,256,2048]{2,1,0:T(8,128)(2,1)}, u32[]{:S(2)}, u32[]{:S(2)}) async-start(bf16[8,256,2048]{2,1,0:T(8,128)(2,1)} %tile.11), calls=%async_computation.5 | async-start | bytes 16777216 | tf_op jit(solution)/shard_map/all_to_all | solution.py:16
  381.6 73.2 %copy-start.16 = (f32[2048]{0:T(1024)S(1)}, f32[2048]{0:T(1024)}, u32[]{:S(2)}) copy-start(f32[2048]{0:T(1024)} %param.20) | copy-start | bytes 24580
  381.6 73.2 %all-gather.12.cloned.1.call-start = ((), (), s32[]{:S(2)}) async-start(), calls=%async_computation.10 | async-start | bytes 2228224 | tf_op jit(solution)/shard_map/all_gather | solution.py:41
  382.3 163.8 %all-gather.14.cloned.1.call-start = ((), (), s32[]{:S(2)}) async-start(), calls=%async_computation.11 | async-start | bytes 4718592 | tf_op jit(solution)/shard_map/all_gather | solution.py:51
  385.7 96.9 %copy-start.10 = (f32[256]{0:T(256)S(1)}, f32[256]{0:T(256)}, u32[]{:S(2)}) copy-start(f32[256]{0:T(256)} %param.24) | copy-start | bytes 3076
  385.7 96.9 %copy-start.11 = (f32[256]{0:T(256)S(1)}, f32[256]{0:T(256)}, u32[]{:S(2)}) copy-start(f32[256]{0:T(256)} %param.23) | copy-start | bytes 3076
  385.7 97.4 %copy-start.6 = (bf16[2,128,128]{2,1,0:T(8,128)(2,1)S(1)}, bf16[2,128,128]{2,1,0:T(8,128)(2,1)}, u32[]{:S(2)}) copy-start(bf16[2,128,128]{2,1,0:T(8,128)(2,1)} %param.25) | copy-start | bytes 196612
  385.7 97.4 %copy-start.12 = (f32[2,128]{1,0:T(2,128)S(1)}, f32[2,128]{1,0:T(2,128)}, u32[]{:S(2)}) copy-start(f32[2,128]{1,0:T(2,128)} %param.26) | copy-start | bytes 3076
  512.3 37.1 %copy-start.17 = (f32[2048]{0:T(1024)S(1)}, f32[2048]{0:T(1024)}, u32[]{:S(2)}) copy-start(f32[2048]{0:T(1024)} %param.16) | copy-start | bytes 24580
  549.5 23.6 %slice-start = ((s8[14680064]{0:T(1024)(128)(4,1)}), s8[4194304]{0:T(1024)(128)(4,1)S(1)}, s32[]{:S(2)}) async-start(s8[14680064]{0:T(1024)(128)(4,1)} %bitcast.99), calls=%async_computation.12 | async-start | bytes 8388608
  549.5 23.6 %slice-start.1 = ((s8[14680064]{0:T(1024)(128)(4,1)}), s8[4194304]{0:T(1024)(128)(4,1)S(1)}, s32[]{:S(2)}) async-start(s8[14680064]{0:T(1024)(128)(4,1)} %bitcast.99), calls=%async_computation.13 | async-start | bytes 8388608
  553.6 19.6 %slice-start.2 = ((s8[14680064]{0:T(1024)(128)(4,1)}), s8[4194304]{0:T(1024)(128)(4,1)S(1)}, s32[]{:S(2)}) async-start(s8[14680064]{0:T(1024)(128)(4,1)} %bitcast.99), calls=%async_computation.14 | async-start | bytes 8388608
  553.6 19.6 %slice-start.3 = ((s8[14680064]{0:T(1024)(128)(4,1)}), s8[2097152]{0:T(1024)(128)(4,1)S(1)}, s32[]{:S(2)}) async-start(s8[14680064]{0:T(1024)(128)(4,1)} %bitcast.99), calls=%async_computation.15 | async-start | bytes 4194304
  (6 other events, 19.6 us)
Sparse Core Ops, SparseCore 0:
  9.2 38.7 all-gather.5
  49.7 75.7 all-gather.7
  337.7 34.8 all-gather.9
  383.9 70.9 all-gather.11
  514.8 31.2 all-gather.13
